TPU v7x, 32 devices: a whole 2x2x4 slice. The times are simulated.
32 devices in a mesh: ep: 8 (over z, x), tp: 4 (over y, core).
Axes of the slice: x: 2, y: 2, z: 4, core: 2. Of those that a mesh axis runs over, the one named last changes fastest.
Arguments:
- mix_query: bfloat16 [2048, 2048], P('ep', 'tp'), may hold values from -6 to 6
- forget_input: bfloat16 [2048, 2048], P('ep', 'tp'), may hold values from -6 to 6
- mix_value: bfloat16 [2048, 2048], P('ep', 'tp'), may hold values from -6 to 6
- out_gate_input: bfloat16 [2048, 2048], P('ep', 'tp'), may hold values from -6 to 6
- decay_shift: float32 [2048, 16], P('ep', 'tp'), may hold values from -1.5 to 0
- forget_floor: float32 [2048], P('tp'), may hold values from 0.9 to 1
- head_gain: float32 [128], replicated, may hold values from 0.1 to 1.9
- w_mix_out: bfloat16 [2048, 2048], P(None, 'tp'), may hold values from -0.125 to 0.125
- moe_input: bfloat16 [2048, 2048], P('ep'), may hold values from -6 to 6
- moe_gain: float32 [2048], replicated, may hold values from 0.1 to 1.9
- routes: int32 [2048, 2], P('ep'), may hold values from 0 to 7, all different within a row; in each aligned block of 256 rows (0 to 255, 256 to 511, ...) at most 80 rows name the same one
- route_weight: float32 [2048, 2], P('ep'), may hold values from 0.1 to 1
- w_exp_gate: bfloat16 [8, 2048, 4096], P('ep', None, 'tp'), may hold values from -0.125 to 0.125
- w_exp_up: bfloat16 [8, 2048, 4096], P('ep', None, 'tp'), may hold values from -0.125 to 0.125
- w_exp_down: bfloat16 [8, 4096, 2048], P('ep', 'tp'), may hold values from -0.125 to 0.125
Outputs:
- mixed: bfloat16 [2048, 2048], P('ep', 'tp')
- moe_out: bfloat16 [2048, 2048], P('ep', 'tp')
Inputs may be any that keep to these rules, and one draw needn't show every extreme that they name: `routes`: at most 80 of the rows of one index of ep name one expert, and in every draw some device's rows name one expert exactly 80 times; the experts of a row differ.
All inputs are finite; a program needn't handle non-finite values.
Results may differ from a plain program's by a relative error of at most 0.02.
Values may be sent and summed in bfloat16 or wider, within the bound.
A program may use at most 64 MiB of HBM per device.

v0:
```python
import jax
import jax.numpy as jnp
from jax import lax
from jax.sharding import PartitionSpec as P

TOP_K = 2
eps = 1e-06
highest_precision = lax.Precision.HIGHEST


def carried_in(shard, axis, join, neutral):
    place = lax.axis_index(axis)
    gathered = jax.tree.map(
        lambda a, kind: lax.all_gather(a.astype(kind), axis), shard, (jnp.bfloat16, jnp.bfloat16)
    )
    state = jax.tree.map(lambda a, e: jnp.zeros_like(a) + jnp.asarray(e, a.dtype), shard, neutral)

    def one(turn, state):
        return join(
            state,
            jax.tree.map(
                lambda a, own: lax.dynamic_index_in_dim(a, turn, 0, False).astype(own.dtype),
                gathered,
                shard,
            ),
        )

    return lax.fori_loop(0, place, one, state)


def chain_step(earlier, later):
    return (earlier[0] * later[0], later[0][:, :, None] * earlier[1] + later[1])


def token_mixer(
    mix_query,
    forget_input,
    mix_value,
    out_gate_input,
    decay_shift,
    forget_floor,
    head_gain,
    w_mix_out,
):
    length = mix_query.shape[0]
    heads_here = decay_shift.shape[1]
    head_size = head_gain.shape[0]
    gate_input = forget_input.astype(jnp.float32)
    forget = forget_floor + (1.0 - forget_floor) * jax.nn.sigmoid(gate_input)
    input_gate = (1.0 - forget_floor) * jax.nn.sigmoid(-gate_input)
    log_decay = jnp.log(forget) + jnp.repeat(decay_shift, head_size, axis=1)

    def by_head(array):
        return array.reshape(length, heads_here, head_size).transpose(1, 0, 2)

    running_decay = jnp.cumsum(by_head(log_decay), axis=1)
    query_rows = by_head(mix_query.astype(jnp.float32)) * jnp.exp(running_decay)
    head_keys = by_head(input_gate)
    values = by_head(mix_value.astype(jnp.float32))
    scores = jnp.einsum(
        "htk,hsk->hts", query_rows, head_keys * jnp.exp(-running_decay), precision=highest_precision
    )
    causal = jnp.arange(length)[:, None] >= jnp.arange(length)[None, :]
    scores = jnp.where(causal[None, :, :], scores, 0.0)
    within_block_output = jnp.einsum("hts,hsv->htv", scores, values, precision=highest_precision)
    closing_total = running_decay[:, -1, :]
    carried_over_state = jnp.einsum(
        "gbx,gbi->gxi",
        head_keys * jnp.exp(closing_total[:, None, :] - running_decay),
        values,
        precision=highest_precision,
    )
    incoming_state = carried_in(
        (jnp.exp(closing_total), carried_over_state),
        "ep",
        chain_step,
        (jnp.ones_like(closing_total), jnp.zeros_like(carried_over_state)),
    )[1]
    block_result = within_block_output + jnp.einsum(
        "rsd,rda->rsa", query_rows, incoming_state, precision=highest_precision
    )
    inverse = lax.rsqrt(jnp.mean(block_result * block_result, axis=2, keepdims=True) + eps)
    gated = by_head(jax.nn.silu(out_gate_input.astype(jnp.float32)))
    normed_heads = (block_result * inverse * head_gain * gated).transpose(1, 0, 2)
    head_out = normed_heads.reshape(length, heads_here * head_size).astype(jnp.bfloat16)
    mixed = jnp.dot(
        lax.all_gather(head_out, "tp", axis=1, tiled=True),
        w_mix_out,
        preferred_element_type=jnp.float32,
    )
    return mixed.astype(jnp.bfloat16)


def experts_layer(moe_input, moe_gain, routes, route_weight, w_exp_gate, w_exp_up, w_exp_down):
    row_count = moe_input.shape[0]
    expert_count = lax.axis_size("ep")
    capacity = 5 * row_count * TOP_K // (4 * expert_count)
    token_rows = moe_input.astype(jnp.float32)
    inverse = lax.rsqrt(jnp.mean(token_rows * token_rows, axis=1, keepdims=True) + eps)
    normed = (token_rows * inverse * moe_gain).astype(jnp.bfloat16)
    flat_ids = routes.reshape(-1)
    pair_count = flat_ids.shape[0]
    one_hot = (flat_ids[:, None] == jnp.arange(expert_count, dtype=jnp.int32)[None, :]).astype(
        jnp.int32
    )
    earlier_count = jnp.cumsum(one_hot, axis=0) - one_hot
    ranks = jnp.sum(earlier_count * one_hot, axis=1)
    slot_ids = flat_ids * capacity + ranks
    owners = (
        jnp.zeros((expert_count * capacity,), jnp.int32)
        .at[slot_ids]
        .set(jnp.arange(pair_count, dtype=jnp.int32) // TOP_K)
    )
    filled = (
        jnp.zeros((expert_count * capacity,), jnp.bfloat16)
        .at[slot_ids]
        .set(jnp.ones((pair_count,), jnp.bfloat16))
    )
    outgoing = normed[owners] * filled[:, None]
    w_gate = w_exp_gate[0]
    w_up = w_exp_up[0]
    w_down = w_exp_down[0]
    width = normed.shape[1] // lax.axis_size("tp")
    own_slice = lax.dynamic_slice_in_dim(outgoing, lax.axis_index("tp") * width, width, 1)
    arrived = lax.all_to_all(own_slice, "ep", split_axis=0, concat_axis=0, tiled=True)
    portion = lax.all_gather(arrived, "tp", axis=1, tiled=True)
    gate_sum = jnp.dot(portion, w_gate, preferred_element_type=jnp.float32)
    up_sum = jnp.dot(portion, w_up, preferred_element_type=jnp.float32)
    hidden = (jax.nn.silu(gate_sum) * up_sum).astype(jnp.bfloat16)
    partial_value = jnp.dot(hidden, w_down, preferred_element_type=jnp.float32)
    summed = lax.psum_scatter(
        partial_value.astype(jnp.bfloat16), "tp", scatter_dimension=1, tiled=True
    )
    returned = lax.all_to_all(summed, "ep", split_axis=0, concat_axis=0, tiled=True)
    picked = returned[slot_ids].astype(jnp.float32).reshape(row_count, TOP_K, returned.shape[1])
    combined = jnp.sum(picked * route_weight[:, :, None], axis=1)
    return combined.astype(jnp.bfloat16)


def body(
    mix_query,
    forget_input,
    mix_value,
    out_gate_input,
    decay_shift,
    forget_floor,
    head_gain,
    w_mix_out,
    moe_input,
    moe_gain,
    routes,
    route_weight,
    w_exp_gate,
    w_exp_up,
    w_exp_down,
):
    mixed = token_mixer(
        mix_query,
        forget_input,
        mix_value,
        out_gate_input,
        decay_shift,
        forget_floor,
        head_gain,
        w_mix_out,
    )
    moe_out = experts_layer(
        moe_input, moe_gain, routes, route_weight, w_exp_gate, w_exp_up, w_exp_down
    )
    return (mixed, moe_out)


def solution(mesh):
    placed = (
        P("ep", "tp"),
        P("ep", "tp"),
        P("ep", "tp"),
        P("ep", "tp"),
        P("ep", "tp"),
        P("tp"),
        P(),
        P(None, "tp"),
        P("ep", None),
        P(),
        P("ep", None),
        P("ep", None),
        P("ep", None, "tp"),
        P("ep", None, "tp"),
        P("ep", "tp", None),
    )
    return jax.shard_map(
        body, mesh=mesh, in_specs=placed, out_specs=(P("ep", "tp"), P("ep", "tp")), check_vma=False
    )
```

profile of v0, /device:TPU:0, one launch (start us, length us, event | category | flops | bytes accessed | tf_op | source)
XLA Modules:
  0.0 189.2 jit_solution(8927491651452208620)
XLA Ops:
  7.2 0.0 copy-start
  7.2 0.0 all-gather.8.cloned.1.call-start
  7.2 0.9 copy.108
  8.2 0.1 eq.29
  8.3 0.1 eq.25
  8.5 0.7 broadcast_multiply_fusion
  9.2 1.1 reduce-window.16
  10.3 0.2 slice_reduce_fusion
  10.6 0.1 copy.107
  10.7 0.1 mul.149
  10.9 0.1 fusion.42
  11.0 2.4 %scatter_custom_fusion = s32[640]{0:T(1024)S(1)} fusion(s32[512]{0:T(512)S(1)} %bitcast.123, s32[512]{0:T(512)S(1)} %add_select_fusion, s32[]{:T(128)} %constant.68.clone.1), kind=kCustom, calls=%fused_computation.82 | custom fusion | bytes 2564 | tf_op jit(solution)/shard_map/scatter | solution.py:112
  13.5 1.5 fusion.9
  15.0 1.5 fusion.11
  16.5 4.1 %gather_fusion = bf16[640,2048]{1,0:T(8,128)(2,1)} fusion(bf16[256,2048]{1,0:T(8,128)(2,1)S(1)} %fusion.11, s32[1024]{0:T(1024)S(1)} %pad_clamp_fusion.1), kind=kCustom, calls=%fused_computation | custom fusion | bytes 5245440 | tf_op jit(solution)/shard_map/gather | solution.py:119
  20.6 3.8 %scatter_custom_fusion.1 = bf16[640]{0:T(1024)(128)(2,1)S(1)} fusion(s32[512]{0:T(512)S(1)} %bitcast.124, bf16[512]{0:T(512)(128)(2,1)S(1)} %broadcast.119, bf16[]{:T(256)} %constant.79.clone.1), kind=kCustom, calls=%fused_computation.87 | custom fusion | bytes 1282 | tf_op jit(solution)/shard_map/scatter | solution.py:117
  24.4 1.3 dynamic-slice_multiply_fusion
  25.7 24.9 %all_to_all.24 = bf16[8,80,512]{2,1,0:T(8,128)(2,1)} all-to-all(bf16[8,80,512]{2,1,0:T(8,128)(2,1)S(1)} %bitcast.112), channel_id=1, replica_groups=mesh['ep'=8,'tp'=4] {'ep'}, dimensions={0} | all-to-all | bytes 1310720 | tf_op jit(solution)/shard_map/all_to_all | solution.py:125
  50.5 0.0 all-gather.8.cloned.1.call-update
  50.6 0.0 all-gather.10.cloned.1.call-start
  50.6 0.0 copy-done.2
  50.6 0.1 copy.92
  50.8 0.0 copy-done.4
  50.8 0.0 copy-done.5
  50.8 1.1 fusion.25
  51.9 0.2 copy.93
  52.1 0.4 fusion.34
  52.5 0.2 broadcast_add_fusion
  52.8 1.1 copy.144
  53.9 2.2 %copy.97 = f32[256,4,128]{2,1,0:T(4,128)} copy(f32[256,4,128]{0,2,1:T(8,128)} %bitcast.114) | data formatting | bytes 1048576 | tf_op jit(solution)/shard_map/reshape | solution.py:54
  56.1 1.1 copy.90
  57.2 0.9 copy.91
  58.1 0.7 slice_bitcast_fusion.1
  58.8 2.8 %bitcast_multiply_fusion.2 = (f32[4,256,128]{2,0,1:T(4,128)}, f32[4,256,128]{2,0,1:T(4,128)S(1)}, f32[4,256,128]{2,0,1:T(4,128)S(1)}) fusion(f32[256,4,128]{2,1,0:T(4,128)} %copy.97, f32[4,128,256]{1,2,0:T(8,128)S(1)} %bitcast.110, f32[4,128]{1,0:T(4,128)S(1)} %get-tuple-element.60, f32[256,4,128]{2,1,0:T(4,128)} %copy.91), kind=kLoop, calls=%fused_computation.47 | loop fusion | flops 655360 | bytes 3147776 | tf_op jit(solution)/shard_map/mul | solution.py:61
  61.5 0.0 copy-done.1
  61.5 1.3 convolution_convert_fusion.1
  62.8 0.0 all-gather.10.cloned.1.call-update
  62.9 0.2 reduce-scatter.2.cloned.1.call-start
  63.1 11.9 %all-gather.8.cloned.1.call-done = bf16[640,2048]{1,0:T(8,128)(2,1)} async-done(((bf16[640,512]{1,0:T(8,128)(2,1)}), bf16[640,2048]{1,0:T(8,128)(2,1)}) %all-gather.8.cloned.1.call-update) | async-done | bytes 2621456 | tf_op jit(solution)/shard_map/all_gather | solution.py:126
  75.0 7.4 %fusion.2 = f32[640,1024]{1,0:T(8,128)} fusion(bf16[640,2048]{1,0:T(8,128)(2,1)} %all-gather.8.cloned.1.call-done, bf16[1,2048,1024]{2,1,0:T(8,128)(2,1)} %param.30), kind=kOutput, calls=%fused_computation.8 | convolution fusion | flops 2684354560 | bytes 9437184 | tf_op jit(solution)/shard_map/dot_general | solution.py:128
  82.3 12.5 %fusion.6 = bf16[640,2048]{1,0:T(8,128)(2,1)} fusion(bf16[1,1024,2048]{2,1,0:T(8,128)(2,1)} %param.31, f32[640,1024]{1,0:T(8,128)} %fusion.2, bf16[640,2048]{1,0:T(8,128)(2,1)} %all-gather.8.cloned.1.call-done, bf16[1,2048,1024]{2,1,0:T(8,128)(2,1)} %param.29), kind=kOutput, calls=%fused_computation.12 | convolution fusion | flops 5373952000 | bytes 16252928 | tf_op jit(solution)/shard_map/dot_general | solution.py:130
  94.8 0.0 reduce-scatter.2.cloned.1.call-update
  94.8 0.0 all-gather.6.cloned.1.call-start
  94.9 26.4 %all-gather = bf16[32,1,128]{2,1,0:T(2,128)(2,1)S(1)} all-gather(bf16[4,1,128]{2,1,0:T(2,128)(2,1)S(1)} %copy.102), channel_id=2, replica_groups=mesh['ep'=8,'tp'=4] {'ep'}, dimensions={0}, use_global_device_ids=true | all-gather | bytes 9216 | tf_op jit(solution)/shard_map/all_gather | solution.py:14
  121.3 0.0 copy-done.3
  121.3 0.1 copy.106
  121.5 0.1 convert_multiply_fusion.2
  121.6 3.0 %convolution_select_fusion = f32[4,256,256]{2,1,0:T(8,128)} fusion(f32[4,256,128]{2,0,1:T(4,128)} %get-tuple-element.57, pred[256,256]{1,0:T(8,128)(4,1)S(1)} %iota_compare_fusion, f32[4,256,128]{2,0,1:T(4,128)S(1)} %get-tuple-element.59), kind=kOutput, calls=%fused_computation.19 | convolution fusion | flops 402915328 | bytes 2162688 | tf_op jit(solution)/shard_map/htk,hsk->hts/dot_general | solution.py:60
  124.7 0.0 copy-start.7
  124.7 0.6 fusion.36
  125.4 0.0 copy-start.6
  125.4 2.2 %multiply_reduce_fusion.1 = (f32[4,256]{1,0:T(4,128)S(1)}, f32[4,256,128]{1,2,0:T(8,128)S(1)}) fusion(f32[4,256,128]{1,2,0:T(8,128)S(1)} %fusion.36, f32[4,256,256]{2,1,0:T(8,128)} %convolution_select_fusion, bf16[256,512]{1,0:T(8,128)(2,1)} %param.19), kind=kOutput, calls=%fused_computation.54 | convolution fusion | flops 403045376 | bytes 2363392 | tf_op jit(solution)/shard_map/hts,hsv->htv/dot_general | solution.py:65
  127.6 0.0 copy-done.7
  127.6 0.8 fusion.31
  128.4 0.0 all-gather.6.cloned.1.call-update
  128.4 25.2 %reduce-scatter.2.cloned.1.call-done = bf16[640,512]{1,0:T(8,128)(2,1)} async-done(((bf16[640,2048]{1,0:T(8,128)(2,1)}), bf16[640,512]{1,0:T(8,128)(2,1)}) %reduce-scatter.2.cloned.1.call-update) | async-done | bytes 655376 | tf_op jit(solution)/shard_map/reduce_scatter | solution.py:131
  153.7 5.5 %all-to-all-start.1 = ((bf16[8,80,512]{2,1,0:T(8,128)(2,1)}), bf16[8,80,512]{2,1,0:T(8,128)(2,1)S(1)}, u32[]{:S(2)}, u32[]{:S(2)}) async-start(bf16[8,80,512]{2,1,0:T(8,128)(2,1)} %bitcast.119), calls=%async_computation.2 | async-start | bytes 1310720 | tf_op jit(solution)/shard_map/all_to_all | solution.py:134
  159.2 0.1 copy.110
  159.3 13.1 %all-gather.6.cloned.1.call-done = bf16[256,2048]{0,1:T(8,128)(2,1)} async-done(((bf16[256,512]{0,1:T(8,128)(2,1)}), bf16[256,2048]{0,1:T(8,128)(2,1)}) %all-gather.6.cloned.1.call-update) | async-done | bytes 1048592 | tf_op jit(solution)/shard_map/all_gather | solution.py:87
  172.4 2.7 %convolution_convert_fusion = bf16[256,512]{1,0:T(8,128)(2,1)} fusion(bf16[256,2048]{0,1:T(8,128)(2,1)} %all-gather.6.cloned.1.call-done, bf16[2048,512]{1,0:T(8,128)(2,1)S(1)} %copy-done), kind=kOutput, calls=%fused_computation.21 | convolution fusion | flops 537001984 | bytes 3407872 | tf_op jit(solution)/shard_map/dot_general | solution.py:86
  175.0 1.3 all-to-all-done.1
  176.3 2.6 %gather_fusion.1 = bf16[512,512]{1,0:T(8,128)(2,1)} fusion(bf16[640,512]{1,0:T(8,128)(2,1)S(1)} %bitcast.108, s32[1024]{0:T(1024)S(1)} %pad_clamp_fusion), kind=kCustom, calls=%fused_computation.1 | custom fusion | bytes 1050624 | tf_op jit(solution)/shard_map/gather | solution.py:135
  178.9 1.7 reshape.158
  180.6 2.1 %multiply_reduce_fusion = bf16[256,512]{1,0:T(8,128)(2,1)} fusion(f32[256,2,512]{2,1,0:T(2,128)S(1)} %reshape.158, f32[256,2]{1,0:T(8,128)S(1)} %copy.110), kind=kLoop, calls=%fused_computation.23 | loop fusion | flops 393216 | bytes 1312768 | tf_op jit(solution)/shard_map/reduce_sum | solution.py:136
  (29 shorter events, 0.3 us)
Async XLA Ops:
  7.2 165.2 %copy-start = (bf16[2048,512]{1,0:T(8,128)(2,1)S(1)}, bf16[2048,512]{1,0:T(8,128)(2,1)}, u32[]{:S(2)}) copy-start(bf16[2048,512]{1,0:T(8,128)(2,1)} %param.24) | copy-start | bytes 6291460
  7.2 67.8 %all-gather.8.cloned.1.call-start = ((), (), s32[]{:S(2)}) async-start(), calls=%async_computation.4 | async-start | bytes 3276800 | tf_op jit(solution)/shard_map/all_gather | solution.py:126
  20.6 30.0 %copy-start.2 = (bf16[256,512]{1,0:T(8,128)(2,1)S(1)}, bf16[256,512]{1,0:T(8,128)(2,1)}, u32[]{:S(2)}) copy-start(bf16[256,512]{1,0:T(8,128)(2,1)} %param.18) | copy-start | bytes 786436
  20.6 30.2 %copy-start.4 = (f32[512]{0:T(512)S(1)}, f32[512]{0:T(512)}, u32[]{:S(2)}) copy-start(f32[512]{0:T(512)} %param.22) | copy-start | bytes 6148
  20.6 30.2 %copy-start.5 = (f32[256,4]{0,1:T(4,128)S(1)}, f32[256,4]{0,1:T(4,128)}, u32[]{:S(2)}) copy-start(f32[256,4]{0,1:T(4,128)} %param.21) | copy-start | bytes 12292
  50.6 74.1 %all-gather.10.cloned.1.call-start = ((), (), s32[]{:S(2)}) async-start(), calls=%async_computation.6 | async-start | bytes 1179648 | tf_op jit(solution)/shard_map/all_gather | solution.py:14
  53.9 7.6 %copy-start.1 = (bf16[256,512]{1,0:T(8,128)(2,1)S(1)}, bf16[256,512]{1,0:T(8,128)(2,1)}, u32[]{:S(2)}) copy-start(bf16[256,512]{1,0:T(8,128)(2,1)} %param.19) | copy-start | bytes 786436
  62.9 90.8 %reduce-scatter.2.cloned.1.call-start = ((), (), s32[]{:S(2)}) async-start(), calls=%async_computation.5 | async-start | bytes 3276800 | tf_op jit(solution)/shard_map/reduce_scatter | solution.py:131
  94.8 26.5 %copy-start.3 = (bf16[256,512]{1,0:T(8,128)(2,1)S(1)}, bf16[256,512]{1,0:T(8,128)(2,1)}, u32[]{:S(2)}) copy-start(bf16[256,512]{1,0:T(8,128)(2,1)} %param.20) | copy-start | bytes 786436
  94.8 77.6 %all-gather.6.cloned.1.call-start = ((), (), s32[]{:S(2)}) async-start(), calls=%async_computation.3 | async-start | bytes 1310720 | tf_op jit(solution)/shard_map/all_gather | solution.py:87
  124.7 2.9 %copy-start.7 = (f32[128]{0:T(128)S(1)}, f32[128]{0:T(128)}, u32[]{:S(2)}) copy-start(f32[128]{0:T(128)} %param.23) | copy-start | bytes 1540
  125.4 33.8 %copy-start.6 = (f32[256,2]{0,1:T(2,128)S(1)}, f32[256,2]{0,1:T(2,128)}, u32[]{:S(2)}) copy-start(f32[256,2]{0,1:T(2,128)} %param.28) | copy-start | bytes 6148
  153.7 22.6 %all-to-all-start.1 = ((bf16[8,80,512]{2,1,0:T(8,128)(2,1)}), bf16[8,80,512]{2,1,0:T(8,128)(2,1)S(1)}, u32[]{:S(2)}, u32[]{:S(2)}) async-start(bf16[8,80,512]{2,1,0:T(8,128)(2,1)} %bitcast.119), calls=%async_computation.2 | async-start | bytes 1310720 | tf_op jit(solution)/shard_map/all_to_all | solution.py:134
Sparse Core Ops, SparseCore 0:
  50.7 24.2 all-gather.7
  77.7 40.3 all-gather.9
  120.5 33.0 reduce-scatter.1
  155.7 16.6 all-gather.5
where the time goes:
time: 190 us; the launch traced here: 189 us
  waiting for transfers between devices  51.5 us (27%)
  blocking collectives  51.3 us (27%)
  matrix products  29.7 us (16%)
  local copies, waits for them, and re-layouts  22.4 us (12%)
  other arithmetic  14.5 us (8%)
  between operations  14 us (7%)
  starting transfers between devices  5.83 us (3%)
    all_gather x1, blocking collectives, carried_in(): lax.all_gather(a.astype(kind), axis)  26.4 us
    reduce_scatter x1, waiting for transfers between devices, experts_layer(): lax.psum_scatter(partial_value.astype(jnp.bfloat16), 'tp', scatter_dimens...  25.2 us
    all_to_all x1, blocking collectives, experts_layer(): lax.all_to_all(own_slice, 'ep', split_axis=0, concat_axis=0, tiled=True)  24.9 us
    all_gather x1, waiting for transfers between devices, token_mixer(): lax.all_gather(head_out, 'tp', axis=1, tiled=True)  13.1 us
    dot_general x1, matrix products, experts_layer(): partial_value = jnp.dot(hidden, w_down, preferred_element_type=jnp.float32)  12.5 us
    all_gather x1, waiting for transfers between devices, experts_layer(): portion = lax.all_gather(arrived, 'tp', axis=1, tiled=True)  11.9 us
    dot_general x1, matrix products, experts_layer(): up_sum = jnp.dot(portion, w_up, preferred_element_type=jnp.float32)  7.36 us
    all_to_all x1, starting transfers between devices, experts_layer(): lax.all_to_all(summed, 'ep', split_axis=0, concat_axis=0, tiled=True)  5.49 us
  transfers between devices with their start and end apart: 5, of which 4 were waited for; matrix products, arithmetic and copies ran while one was open for 22% of the time, Pallas kernels for 0%

commit v1 on v0

--- a/solution.py
+++ b/solution.py
@@ -123,7 +123,12 @@
     width = normed.shape[1] // lax.axis_size("tp")
     own_slice = lax.dynamic_slice_in_dim(outgoing, lax.axis_index("tp") * width, width, 1)
     arrived = lax.all_to_all(own_slice, "ep", split_axis=0, concat_axis=0, tiled=True)
-    portion = lax.all_gather(arrived, "tp", axis=1, tiled=True)
+    ring = [arrived]
+    for hop in range(3):
+        ring.append(lax.ppermute(ring[-1], "tp", [(dev, (dev + 1) % 4) for dev in range(4)]))
+    portion = jnp.roll(
+        jnp.concatenate(ring[::-1], axis=1), (lax.axis_index("tp") + 1) * ring[0].shape[1], axis=1
+    )
     gate_sum = jnp.dot(portion, w_gate, preferred_element_type=jnp.float32)
     up_sum = jnp.dot(portion, w_up, preferred_element_type=jnp.float32)
     hidden = (jax.nn.silu(gate_sum) * up_sum).astype(jnp.bfloat16)

time: 190 us -> 182 us (0.958)
  waiting for transfers between devices: 51.5 us -> 28.2 us
  local copies, waits for them, and re-layouts: 22.4 us -> 34.5 us
  starting transfers between devices: 5.83 us -> 9.96 us
  matrix products: 29.7 us -> 26.4 us
  between operations: 14 us -> 15.9 us
    reduce_scatter x1, waiting for transfers between devices: 25.2 us -> 0.03 us  [experts_layer(): lax.psum_scatter(partial_value.astype(jnp.bfloat16), 'tp', scatter_dimens...]
    ppermute x0 -> x3, waiting for transfers between devices: none -> 15.2 us  [experts_layer(): lax.ppermute(ring[-1], 'tp', [(dev, (dev + 1) % 4) for dev in range(4)])]
    all_gather x1 -> x0, waiting for transfers between devices: 11.9 us -> none  [experts_layer(): portion = lax.all_gather(arrived, 'tp', axis=1, tiled=True)]
    unnamed x22 -> x33, local copies, waits for them, and re-layouts: 2.49 us -> 13.7 us
    all_to_all x1, starting transfers between devices: 5.49 us -> 9.65 us  [experts_layer(): lax.all_to_all(summed, 'ep', split_axis=0, concat_axis=0, tiled=True)]
    dot_general x1, matrix products: 7.36 us -> 4.47 us  [experts_layer(): gate_sum = jnp.dot(portion, w_gate, preferred_element_type=jnp.float32)]
  transfers between devices with their start and end apart: 5 -> 7, of which waited for: 4 -> 5; matrix products, arithmetic and copies ran while one was open for 22% -> 27% of each run, Pallas kernels for 0% -> 0%
where the time goes in v1:
time: 182 us; the launch traced here: 181 us
  blocking collectives  51 us (28%)
  local copies, waits for them, and re-layouts  34.5 us (19%)
  waiting for transfers between devices  28.2 us (15%)
  matrix products  26.4 us (15%)
  between operations  15.9 us (9%)
  other arithmetic  15 us (8%)
  starting transfers between devices  9.96 us (5%)
    all_gather x1, blocking collectives, carried_in(): lax.all_gather(a.astype(kind), axis)  26.3 us
    all_to_all x1, blocking collectives, experts_layer(): lax.all_to_all(own_slice, 'ep', split_axis=0, concat_axis=0, tiled=True)  24.7 us
    ppermute x3, waiting for transfers between devices, experts_layer(): lax.ppermute(ring[-1], 'tp', [(dev, (dev + 1) % 4) for dev in range(4)])  15.2 us
    unnamed x33, local copies, waits for them, and re-layouts  13.7 us
    dot_general x1, matrix products, experts_layer(): partial_value = jnp.dot(hidden, w_down, preferred_element_type=jnp.float32)  12.2 us
    all_gather x1, waiting for transfers between devices, token_mixer(): lax.all_gather(head_out, 'tp', axis=1, tiled=True)  11.9 us
    all_to_all x1, starting transfers between devices, experts_layer(): lax.all_to_all(summed, 'ep', split_axis=0, concat_axis=0, tiled=True)  9.65 us
    dot_general x1, matrix products, experts_layer(): gate_sum = jnp.dot(portion, w_gate, preferred_element_type=jnp.float32)  4.47 us
  transfers between devices with their start and end apart: 7, of which 5 were waited for; matrix products, arithmetic and copies ran while one was open for 27% of the time, Pallas kernels for 0%

profile of v1, /device:TPU:0, one launch (start us, length us, event | category | flops | bytes accessed | tf_op | source)
XLA Modules:
  0.0 181.1 jit_solution(4565839561469484421)
XLA Ops:
  8.0 0.0 copy-start
  8.0 0.0 all-gather.7.cloned.1.call-start
  8.1 0.9 copy.108
  9.0 0.1 eq.32
  9.2 0.1 eq.28
  9.3 0.7 broadcast_multiply_fusion
  10.0 1.1 reduce-window.16
  11.2 0.2 slice_reduce_fusion
  11.4 0.1 copy.107
  11.6 0.1 mul.152
  11.7 0.1 fusion.48
  11.8 2.4 %scatter_custom_fusion = s32[640]{0:T(1024)S(1)} fusion(s32[512]{0:T(512)S(1)} %bitcast.123, s32[512]{0:T(512)S(1)} %add_select_fusion, s32[]{:T(128)} %constant.87.clone.1), kind=kCustom, calls=%fused_computation.92 | custom fusion | bytes 2564 | tf_op jit(solution)/shard_map/scatter | solution.py:112
  14.3 1.5 fusion.11
  15.8 1.5 fusion.13
  17.4 4.1 %gather_fusion = bf16[640,2048]{1,0:T(8,128)(2,1)} fusion(bf16[256,2048]{1,0:T(8,128)(2,1)S(1)} %fusion.13, s32[1024]{0:T(1024)S(1)} %pad_clamp_fusion.1), kind=kCustom, calls=%fused_computation | custom fusion | bytes 5245440 | tf_op jit(solution)/shard_map/gather | solution.py:119
  21.5 3.8 %scatter_custom_fusion.1 = bf16[640]{0:T(1024)(128)(2,1)S(1)} fusion(s32[512]{0:T(512)S(1)} %bitcast.124, bf16[512]{0:T(512)(128)(2,1)S(1)} %broadcast.123, bf16[]{:T(256)} %constant.98.clone.1), kind=kCustom, calls=%fused_computation.97 | custom fusion | bytes 1282 | tf_op jit(solution)/shard_map/scatter | solution.py:117
  25.2 1.3 dynamic-slice_multiply_fusion
  26.5 24.7 %all_to_all.24 = bf16[8,80,512]{2,1,0:T(8,128)(2,1)S(1)} all-to-all(bf16[8,80,512]{2,1,0:T(8,128)(2,1)S(1)} %bitcast.112), channel_id=1, replica_groups=mesh['ep'=8,'tp'=4] {'ep'}, dimensions={0} | all-to-all | bytes 1310720 | tf_op jit(solution)/shard_map/all_to_all | solution.py:125
  51.3 1.1 copy.92
  52.4 1.1 fusion.31
  53.5 1.0 copy.93
  54.5 6.9 %collective-permute-done = bf16[640,512]{1,0:T(8,128)(2,1)} collective-permute-done((bf16[640,512]{1,0:T(8,128)(2,1)S(1)}, bf16[640,512]{1,0:T(8,128)(2,1)}, u32[]{:S(2)}, u32[]{:S(2)}) %collective-permute-start) | collective-permute-done | bytes 655392 | tf_op jit(solution)/shard_map/ppermute | solution.py:128
  61.4 1.5 fusion.40
  62.9 0.2 broadcast_add_fusion
  63.2 0.3 copy.144
  63.5 8.2 %collective-permute-done.1 = bf16[640,512]{1,0:T(8,128)(2,1)} collective-permute-done((bf16[640,512]{1,0:T(8,128)(2,1)}, bf16[640,512]{1,0:T(8,128)(2,1)}, u32[]{:S(2)}, u32[]{:S(2)}) %collective-permute-start.1) | collective-permute-done | bytes 655392 | tf_op jit(solution)/shard_map/ppermute | solution.py:128
  71.7 2.0 %copy.97 = f32[256,4,128]{2,1,0:T(4,128)} copy(f32[256,4,128]{0,2,1:T(8,128)} %bitcast.114) | data formatting | bytes 1048576 | tf_op jit(solution)/shard_map/reshape | solution.py:54
  73.8 1.8 copy.90
  75.6 1.9 %copy.91 = f32[256,4,128]{2,1,0:T(4,128)} copy(bf16[256,4,128]{0,2,1:T(8,128)(2,1)} %bitcast.118) | data formatting | bytes 786432 | tf_op jit(solution)/shard_map/transpose | solution.py:54
  77.5 2.8 %bitcast_multiply_fusion.2 = (f32[4,256,128]{2,0,1:T(4,128)}, f32[4,256,128]{2,0,1:T(4,128)S(1)}, f32[4,256,128]{2,0,1:T(4,128)}) fusion(f32[256,4,128]{2,1,0:T(4,128)} %copy.97, f32[4,128,256]{1,2,0:T(8,128)S(1)} %bitcast.111, f32[4,128]{1,0:T(4,128)S(1)} %get-tuple-element.60, f32[256,4,128]{2,1,0:T(4,128)} %copy.91), kind=kLoop, calls=%fused_computation.49 | loop fusion | flops 655360 | bytes 3147776 | tf_op jit(solution)/shard_map/mul | solution.py:61
  80.3 1.3 convolution_convert_fusion.1
  81.6 0.0 all-gather.7.cloned.1.call-update
  81.6 0.2 reduce-scatter.2.cloned.1.call-start
  81.9 0.2 collective-permute-done.2
  82.0 1.2 constant_dynamic-update-slice_fusion.7
  83.2 1.2 constant_dynamic-update-slice_fusion.6
  84.4 1.3 constant_dynamic-update-slice_fusion.5
  85.7 0.1 constant_dynamic-update-slice_fusion.4
  85.8 1.2 constant_dynamic-update-slice_fusion.3
  87.0 1.2 constant_dynamic-update-slice_fusion.2
  88.2 1.2 constant_dynamic-update-slice_fusion.1
  89.4 0.1 constant_dynamic-update-slice_fusion
  89.5 2.3 %copy-done.4 = bf16[640,4096]{1,0:T(8,128)(2,1)} copy-done((bf16[640,4096]{1,0:T(8,128)(2,1)}, bf16[640,4096]{1,0:T(8,128)(2,1)S(1)}, u32[]{:S(2)}) %copy-start.4) | copy-done | bytes 5242904
  91.8 4.5 %fusion.4 = f32[640,1024]{1,0:T(8,128)} fusion(bf16[1,2048,1024]{2,1,0:T(8,128)(2,1)S(1)} %copy-done.9, bf16[640,4096]{1,0:T(8,128)(2,1)S(1)} %constant_dynamic-update-slice_fusion, s32[]{:T(128)S(6)} %select_n.53), kind=kOutput, calls=%fused_computation.10 | convolution fusion | flops 2684354560 | bytes 9437188 | tf_op jit(solution)/shard_map/dot_general | solution.py:132
  96.2 12.2 %fusion.6 = bf16[640,2048]{1,0:T(8,128)(2,1)} fusion(bf16[1,1024,2048]{2,1,0:T(8,128)(2,1)} %param.31, f32[640,1024]{1,0:T(8,128)} %fusion.4, bf16[1,2048,1024]{2,1,0:T(8,128)(2,1)} %param.30, bf16[640,4096]{1,0:T(8,128)(2,1)} %copy-done.4, s32[]{:T(128)S(6)} %select_n.53), kind=kOutput, calls=%fused_computation.12 | convolution fusion | flops 5373952000 | bytes 16252932 | tf_op jit(solution)/shard_map/dot_general | solution.py:135
  108.5 0.0 reduce-scatter.2.cloned.1.call-update
  108.5 0.0 all-gather.5.cloned.1.call-start
  108.5 26.3 %all-gather = bf16[32,1,128]{2,1,0:T(2,128)(2,1)S(1)} all-gather(bf16[4,1,128]{2,1,0:T(2,128)(2,1)S(1)} %copy.102), channel_id=2, replica_groups=mesh['ep'=8,'tp'=4] {'ep'}, dimensions={0}, use_global_device_ids=true | all-gather | bytes 9216 | tf_op jit(solution)/shard_map/all_gather | solution.py:14
  134.8 0.1 copy.106
  135.0 0.1 convert_multiply_fusion.2
  135.2 3.1 %convolution_select_fusion = f32[4,256,256]{2,1,0:T(8,128)} fusion(f32[4,256,128]{2,0,1:T(4,128)} %get-tuple-element.57, pred[256,256]{1,0:T(8,128)(4,1)S(1)} %iota_compare_fusion, f32[4,256,128]{2,0,1:T(4,128)S(1)} %copy-done.1), kind=kOutput, calls=%fused_computation.21 | convolution fusion | flops 402915328 | bytes 2162688 | tf_op jit(solution)/shard_map/htk,hsk->hts/dot_general | solution.py:60
  138.3 0.6 fusion.42
  139.0 2.0 %multiply_reduce_fusion.1 = (f32[4,256]{1,0:T(4,128)S(1)}, f32[4,256,128]{1,2,0:T(8,128)S(1)}) fusion(f32[4,256,128]{1,2,0:T(8,128)S(1)} %fusion.42, f32[4,256,256]{2,1,0:T(8,128)} %convolution_select_fusion, bf16[256,512]{1,0:T(8,128)(2,1)} %param.19), kind=kOutput, calls=%fused_computation.56 | convolution fusion | flops 403045376 | bytes 2363392 | tf_op jit(solution)/shard_map/hts,hsv->htv/dot_general | solution.py:65
  141.0 0.8 fusion.37
  141.8 0.0 all-gather.5.cloned.1.call-update
  141.9 0.0 reduce-scatter.2.cloned.1.call-done
  141.9 9.7 %all-to-all-start.1 = ((bf16[8,80,512]{2,1,0:T(8,128)(2,1)}), bf16[8,80,512]{2,1,0:T(8,128)(2,1)S(1)}, u32[]{:S(2)}, u32[]{:S(2)}) async-start(bf16[8,80,512]{2,1,0:T(8,128)(2,1)} %bitcast.119), calls=%async_computation.2 | async-start | bytes 1310720 | tf_op jit(solution)/shard_map/all_to_all | solution.py:139
  151.6 0.1 copy.110
  151.7 11.9 %all-gather.5.cloned.1.call-done = bf16[256,2048]{0,1:T(8,128)(2,1)} async-done(((bf16[256,512]{0,1:T(8,128)(2,1)}), bf16[256,2048]{0,1:T(8,128)(2,1)}) %all-gather.5.cloned.1.call-update) | async-done | bytes 1048592 | tf_op jit(solution)/shard_map/all_gather | solution.py:87
  163.6 2.7 %convolution_convert_fusion = bf16[256,512]{1,0:T(8,128)(2,1)} fusion(bf16[256,2048]{0,1:T(8,128)(2,1)} %all-gather.5.cloned.1.call-done, bf16[2048,512]{1,0:T(8,128)(2,1)S(1)} %copy-done), kind=kOutput, calls=%fused_computation.23 | convolution fusion | flops 537001984 | bytes 3407872 | tf_op jit(solution)/shard_map/dot_general | solution.py:86
  166.3 1.0 all-to-all-done.1
  167.3 2.6 %gather_fusion.1 = bf16[512,512]{1,0:T(8,128)(2,1)} fusion(bf16[640,512]{1,0:T(8,128)(2,1)S(1)} %bitcast.106, s32[1024]{0:T(1024)S(1)} %pad_clamp_fusion), kind=kCustom, calls=%fused_computation.1 | custom fusion | bytes 1050624 | tf_op jit(solution)/shard_map/gather | solution.py:140
  169.9 1.7 reshape.158
  171.6 2.1 %multiply_reduce_fusion = bf16[256,512]{1,0:T(8,128)(2,1)} fusion(f32[256,2,512]{2,1,0:T(2,128)S(1)} %reshape.158, f32[256,2]{1,0:T(8,128)S(1)} %copy.110), kind=kLoop, calls=%fused_computation.25 | loop fusion | flops 393216 | bytes 1312768 | tf_op jit(solution)/shard_map/reduce_sum | solution.py:141
  (44 shorter events, 0.3 us)
Async XLA Ops:
  8.0 155.6 %copy-start = (bf16[2048,512]{1,0:T(8,128)(2,1)S(1)}, bf16[2048,512]{1,0:T(8,128)(2,1)}, u32[]{:S(2)}) copy-start(bf16[2048,512]{1,0:T(8,128)(2,1)} %param.24) | copy-start | bytes 6291460
  8.0 130.3 %all-gather.7.cloned.1.call-start = ((), (), s32[]{:S(2)}) async-start(), calls=%async_computation.5 | async-start | bytes 1179648 | tf_op jit(solution)/shard_map/all_gather | solution.py:14
  17.3 35.0 %copy-start.5 = (f32[512]{0:T(512)S(1)}, f32[512]{0:T(512)}, u32[]{:S(2)}) copy-start(f32[512]{0:T(512)} %param.22) | copy-start | bytes 6148
  17.4 35.0 %copy-start.6 = (f32[256,4]{0,1:T(4,128)S(1)}, f32[256,4]{0,1:T(4,128)}, u32[]{:S(2)}) copy-start(f32[256,4]{0,1:T(4,128)} %param.21) | copy-start | bytes 12292
  51.3 10.1 %collective-permute-start = (bf16[640,512]{1,0:T(8,128)(2,1)S(1)}, bf16[640,512]{1,0:T(8,128)(2,1)}, u32[]{:S(2)}, u32[]{:S(2)}) collective-permute-start(bf16[640,512]{1,0:T(8,128)(2,1)S(1)} %bitcast.107), channel_id=1, source_target_pairs={{0,1},{1,2},{2,3},{3,0},{4,5},{5,6},{6,7},{7,4},{8,9},{9,10},{10,1... | collective-permute-start | bytes 1966088 | tf_op jit(solution)/shard_map/ppermute | solution.py:128
  61.4 10.3 %collective-permute-start.1 = (bf16[640,512]{1,0:T(8,128)(2,1)}, bf16[640,512]{1,0:T(8,128)(2,1)}, u32[]{:S(2)}, u32[]{:S(2)}) collective-permute-start(bf16[640,512]{1,0:T(8,128)(2,1)} %collective-permute-done), channel_id=1, source_target_pairs={{0,1},{1,2},{2,3},{3,0},{4,5},{5,6},{6,7},{7,4},{8,9},{9,10},{10,1... | collective-permute-start | bytes 1966088 | tf_op jit(solution)/shard_map/ppermute | solution.py:128
  62.9 17.4 %copy-start.2 = (bf16[256,512]{1,0:T(8,128)(2,1)S(1)}, bf16[256,512]{1,0:T(8,128)(2,1)}, u32[]{:S(2)}) copy-start(bf16[256,512]{1,0:T(8,128)(2,1)} %param.19) | copy-start | bytes 786436
  71.7 10.3 %collective-permute-start.2 = (bf16[640,512]{1,0:T(8,128)(2,1)}, bf16[640,512]{1,0:T(8,128)(2,1)}, u32[]{:S(2)}, u32[]{:S(2)}) collective-permute-start(bf16[640,512]{1,0:T(8,128)(2,1)} %collective-permute-done.1), channel_id=1, source_target_pairs={{0,1},{1,2},{2,3},{3,0},{4,5},{5,6},{6,7},{7,4},{8,9},{9,10},{10,1... | collective-permute-start | bytes 1966088 | tf_op jit(solution)/shard_map/ppermute | solution.py:128
  81.6 60.3 %reduce-scatter.2.cloned.1.call-start = ((), (), s32[]{:S(2)}) async-start(), calls=%async_computation.4 | async-start | bytes 3276800 | tf_op jit(solution)/shard_map/reduce_scatter | solution.py:136
  84.4 7.4 %copy-start.9 = (bf16[1,2048,1024]{2,1,0:T(8,128)(2,1)S(1)}, bf16[1,2048,1024]{2,1,0:T(8,128)(2,1)}, u32[]{:S(2)}) copy-start(bf16[1,2048,1024]{2,1,0:T(8,128)(2,1)} %param.29) | copy-start | bytes 12582916
  89.4 2.3 %copy-start.4 = (bf16[640,4096]{1,0:T(8,128)(2,1)}, bf16[640,4096]{1,0:T(8,128)(2,1)S(1)}, u32[]{:S(2)}) copy-start(bf16[640,4096]{1,0:T(8,128)(2,1)S(1)} %constant_dynamic-update-slice_fusion) | copy-start | bytes 15728644
  96.2 38.6 %copy-start.3 = (bf16[256,512]{1,0:T(8,128)(2,1)S(1)}, bf16[256,512]{1,0:T(8,128)(2,1)}, u32[]{:S(2)}) copy-start(bf16[256,512]{1,0:T(8,128)(2,1)} %param.20) | copy-start | bytes 786436
  108.5 26.7 %copy-start.1 = (f32[4,256,128]{2,0,1:T(4,128)S(1)}, f32[4,256,128]{2,0,1:T(4,128)}, u32[]{:S(2)}) copy-start(f32[4,256,128]{2,0,1:T(4,128)} %get-tuple-element.59) | copy-start | bytes 1572868
  108.5 55.1 %all-gather.5.cloned.1.call-start = ((), (), s32[]{:S(2)}) async-start(), calls=%async_computation.3 | async-start | bytes 1310720 | tf_op jit(solution)/shard_map/all_gather | solution.py:87
  138.3 2.7 %copy-start.8 = (f32[128]{0:T(128)S(1)}, f32[128]{0:T(128)}, u32[]{:S(2)}) copy-start(f32[128]{0:T(128)} %param.23) | copy-start | bytes 1540
  138.3 13.2 %copy-start.7 = (f32[256,2]{0,1:T(2,128)S(1)}, f32[256,2]{0,1:T(2,128)}, u32[]{:S(2)}) copy-start(f32[256,2]{0,1:T(2,128)} %param.28) | copy-start | bytes 6148
  141.9 25.4 %all-to-all-start.1 = ((bf16[8,80,512]{2,1,0:T(8,128)(2,1)}), bf16[8,80,512]{2,1,0:T(8,128)(2,1)S(1)}, u32[]{:S(2)}, u32[]{:S(2)}) async-start(bf16[8,80,512]{2,1,0:T(8,128)(2,1)} %bitcast.119), calls=%async_computation.2 | async-start | bytes 1310720 | tf_op jit(solution)/shard_map/all_to_all | solution.py:139
Sparse Core Ops, SparseCore 0:
  81.8 39.2 all-gather.6
Sparse Core Ops, SparseCore 1:
  108.6 33.1 reduce-scatter.1
  143.7 19.9 all-gather.4
